TPU v7x, 32 devices: a whole 2x2x4 slice. The times are simulated.
32 devices in a mesh: sp: 8 (over z, x), tp: 4 (over y, core).
Axes of the slice: x: 2, y: 2, z: 4, core: 2. Of those that a mesh axis runs over, the one named last changes fastest.
Arguments:
- x_resid: bfloat16 [1024, 2048], P(('sp', 'tp')), may hold values from -3 to 3
- query_proj: bfloat16 [1024, 2048], P('sp', 'tp'), may hold values from -6 to 6
- projected_key_heads: bfloat16 [1024, 1024], P('sp', 'tp'), may hold values from -6 to 6
- projected_value_heads: bfloat16 [1024, 1024], P('sp', 'tp'), may hold values from -6 to 6
- query_gain: float32 [128], replicated, may hold values from 1.3 to 6.5
- key_norm_gain: float32 [128], replicated, may hold values from 1.3 to 6.5
- out_weight: bfloat16 [2048, 2048], P('tp'), may hold values from -0.125 to 0.125
- ffn_gain: float32 [2048], replicated, may hold values from 0.1 to 1.9
- routing: int32 [1024, 2], P(('sp', 'tp')), may hold values from 0 to 7, all different within a row; in each aligned block of 32 rows (0 to 31, 32 to 63, ...) at most 16 rows name the same one
- route_scores: float32 [1024, 2], P(('sp', 'tp')), may hold values from -6 to 6
- expert_gate: bfloat16 [8, 2048, 4096], P('sp', None, 'tp'), may hold values from -0.125 to 0.125
- expert_up: bfloat16 [8, 2048, 4096], P('sp', None, 'tp'), may hold values from -0.125 to 0.125
- expert_down: bfloat16 [8, 4096, 2048], P('sp', 'tp'), may hold values from -0.09375 to 0.09375
Outputs:
- layer_out: bfloat16 [1024, 2048], P(('sp', 'tp'))
Inputs may be any that keep to these rules, and one draw needn't show every extreme that they name: `routing`: each row names 2 different experts. In each aligned block of 32 rows (the rows of one device) no expert is named by more than 16 rows, a bound that some block reaches.
All inputs are finite; a program needn't handle non-finite values.
Results may differ from a plain program's by a relative error of at most 0.018.
The roundings to bfloat16 on the way count: a program that leaves them out, or rounds other values in their place, can miss the bound.
Values may be sent and summed in bfloat16 or wider, within the bound.
A program may use at most 128 MiB of HBM per device.

v0:
```python
import jax
import jax.numpy as jnp
from jax import lax
from jax.sharding import PartitionSpec as P

HEAD_WIDTH = 128
TOP = 2
GRID_W = 64


NORM_EPS = 1e-06
ROPE_BASE = 10000.0
NEG_LARGE = -1e30


def rms_scale(values, norm_gain):
    return (
        values * lax.rsqrt(jnp.mean(values * values, axis=-1, keepdims=True) + NORM_EPS) * norm_gain
    )


def grid_angles(token_positions, head_size):
    freq_count = head_size // 4
    frequency = ROPE_BASE ** (-jnp.arange(freq_count, dtype=jnp.float32) / freq_count)
    grid_row = (token_positions // GRID_W).astype(jnp.float32)
    grid_col = (token_positions % GRID_W).astype(jnp.float32)
    return (grid_row[:, None] * frequency, grid_col[:, None] * frequency)


def turn_half(values, angles):
    cosine = jnp.cos(angles)[:, None, :]
    sine_part = jnp.sin(angles)[:, None, :]
    leading, trailing = jnp.split(values, 2, axis=-1)
    return jnp.concatenate(
        [leading * cosine - trailing * sine_part, trailing * cosine + leading * sine_part], axis=-1
    )


def normalize_rotate(projected, norm_gain, token_positions, heads):
    length = projected.shape[0]
    values = projected.astype(jnp.float32).reshape(length, heads, -1)
    head_size = values.shape[-1]
    values = rms_scale(values, norm_gain)
    row_angle, col_angle = grid_angles(token_positions, head_size)
    half_size = head_size // 2
    turned = jnp.concatenate(
        [
            turn_half(values[..., :half_size], row_angle),
            turn_half(values[..., half_size:], col_angle),
        ],
        axis=-1,
    )
    return turned.reshape(length, heads * head_size).astype(jnp.bfloat16)


def local(
    x_resid,
    query_proj,
    projected_key_heads,
    projected_value_heads,
    query_gain,
    key_norm_gain,
    out_weight,
    ffn_gain,
    routing,
    route_scores,
    expert_gate,
    expert_up,
    expert_down,
):
    seq_rows = query_proj.shape[0]
    q_heads = query_proj.shape[1] // HEAD_WIDTH
    kv_heads = projected_key_heads.shape[1] // HEAD_WIDTH
    head_groups = q_heads // kv_heads
    token_positions = lax.axis_index("sp") * seq_rows + jnp.arange(seq_rows, dtype=jnp.int32)
    query_rows = normalize_rotate(query_proj, query_gain, token_positions, q_heads)
    rotated_key_rows = normalize_rotate(
        projected_key_heads, key_norm_gain, token_positions, kv_heads
    )
    query_grid = query_rows.reshape(seq_rows, kv_heads, head_groups, HEAD_WIDTH)
    score_scale = HEAD_WIDTH ** (-0.5)
    run_max = jnp.full((kv_heads, head_groups, seq_rows), NEG_LARGE, jnp.float32)
    key_piece = lax.all_gather(rotated_key_rows, "sp", axis=0, tiled=True).reshape(
        -1, kv_heads, HEAD_WIDTH
    )
    value_piece = lax.all_gather(projected_value_heads, "sp", axis=0, tiled=True).reshape(
        -1, kv_heads, HEAD_WIDTH
    )
    scores = (
        jnp.einsum("qhgd,khd->hgqk", query_grid, key_piece, preferred_element_type=jnp.float32)
        * score_scale
    )
    new_max = jnp.maximum(run_max, jnp.max(scores, axis=-1))
    weights = jnp.exp(scores - new_max[..., None])
    new_total = jnp.sum(weights, axis=-1)
    addition = jnp.einsum(
        "hgqk,khd->hgqd",
        weights.astype(jnp.bfloat16),
        value_piece,
        preferred_element_type=jnp.float32,
    )
    attended = (
        (addition / new_total[..., None])
        .transpose(2, 0, 1, 3)
        .reshape(seq_rows, q_heads * HEAD_WIDTH)
        .astype(jnp.bfloat16)
    )
    own_tokens = x_resid.shape[0]
    model_width = x_resid.shape[1]
    row_block = attended
    attn_proj = lax.psum_scatter(
        jnp.dot(row_block, out_weight, preferred_element_type=jnp.float32).astype(jnp.bfloat16),
        "tp",
        scatter_dimension=0,
        tiled=True,
    )
    middle = x_resid.astype(jnp.float32) + attn_proj.astype(jnp.float32)
    normed = rms_scale(middle, ffn_gain).astype(jnp.bfloat16)
    experts_all = lax.axis_size("sp") * expert_gate.shape[0]
    capacity = max(2, 2 * own_tokens * TOP // experts_all)
    flat_expert = routing.reshape(-1)
    one_hot = (flat_expert[:, None] == jnp.arange(experts_all, dtype=jnp.int32)[None, :]).astype(
        jnp.int32
    )
    earlier = jnp.cumsum(one_hot, axis=0) - one_hot
    slot_rank = jnp.sum(earlier * one_hot, axis=1)
    target = flat_expert * capacity + slot_rank
    chooser = (
        jnp.arange(experts_all * capacity, dtype=jnp.int32)[:, None] == target[None, :]
    ).astype(jnp.float32)
    gate_share = jax.nn.softmax(route_scores, axis=-1).reshape(-1)
    picker = jnp.sum(chooser.reshape(experts_all * capacity, own_tokens, TOP), axis=2).astype(
        jnp.bfloat16
    )
    combiner = jnp.sum(
        (chooser * gate_share[None, :]).reshape(experts_all * capacity, own_tokens, TOP), axis=2
    )
    dispatch = (
        jnp.dot(picker, normed, preferred_element_type=jnp.float32)
        .astype(jnp.bfloat16)
        .reshape(experts_all, capacity, model_width)
    )
    gate_matrix = expert_gate[0]
    up_matrix = expert_up[0]
    down_matrix = expert_down[0]
    arrived = lax.all_to_all(dispatch, "sp", split_axis=0, concat_axis=0, tiled=True)
    row_block = lax.all_gather(arrived.reshape(-1, model_width), "tp", axis=0, tiled=True)
    gate_part = jnp.dot(row_block, gate_matrix, preferred_element_type=jnp.float32)
    up_part = jnp.dot(row_block, up_matrix, preferred_element_type=jnp.float32)
    hidden = (jax.nn.silu(gate_part) * up_part).astype(jnp.bfloat16)
    row_block = hidden
    expert_result = lax.psum_scatter(
        jnp.dot(row_block, down_matrix, preferred_element_type=jnp.float32).astype(jnp.bfloat16),
        "tp",
        scatter_dimension=0,
        tiled=True,
    )
    returned = lax.all_to_all(
        expert_result.reshape(-1, capacity, model_width),
        "sp",
        split_axis=0,
        concat_axis=0,
        tiled=True,
    )
    routed = jnp.einsum(
        "st,sd->td",
        combiner,
        returned.reshape(-1, model_width).astype(jnp.float32),
        precision=lax.Precision.HIGHEST,
    )
    return (middle + routed).astype(jnp.bfloat16)


def solution(mesh):
    in_specs = (
        P(("sp", "tp"), None),
        P("sp", "tp"),
        P("sp", "tp"),
        P("sp", "tp"),
        P(),
        P(),
        P("tp", None),
        P(),
        P(("sp", "tp"), None),
        P(("sp", "tp"), None),
        P("sp", None, "tp"),
        P("sp", None, "tp"),
        P("sp", "tp", None),
    )
    out_specs = P(("sp", "tp"), None)
    return jax.shard_map(local, mesh=mesh, in_specs=in_specs, out_specs=out_specs, check_vma=False)
```

profile of v0, /device:TPU:0, one launch (start us, length us, event | category | flops | bytes accessed | tf_op | source)
XLA Modules:
  0.0 216.5 jit_solution(6405185834197170477)
XLA Ops:
  6.5 0.0 copy-start
  6.5 0.0 copy-start.4
  6.5 0.0 copy-start.9
  6.5 0.0 reduce-scatter.3.cloned.1.call-start
  6.6 1.1 reshape.250
  7.6 0.2 multiply_reduce_fusion.2
  7.9 0.9 multiply_multiply_fusion.1
  8.7 0.5 multiply_cosine_fusion.1
  9.3 0.5 subtract_convert_fusion.3
  9.8 0.4 pad_maximum_fusion.1
  10.2 0.1 copy.54
  10.3 0.0 copy-done.4
  10.3 0.1 reshape.252
  10.4 0.2 multiply_reduce_fusion.1
  10.6 0.0 copy-start.5
  10.7 0.0 copy-done.9
  10.7 0.2 multiply_multiply_fusion
  10.9 0.5 subtract_convert_fusion.1
  11.4 0.4 pad_maximum_fusion
  11.8 29.6 %all_gather.9 = bf16[1024,256]{0,1:T(8,128)(2,1)S(1)} all-gather(bf16[128,256]{0,1:T(8,128)(2,1)S(1)} %bitcast.66), channel_id=1, replica_groups=mesh['sp'=8,'tp'=4] {'sp'}, dimensions={0}, use_global_device_ids=true | all-gather | bytes 589824 | tf_op jit(solution)/shard_map/all_gather | solution.py:83
  41.4 0.0 copy-done.5
  41.4 31.4 %all_gather.10 = bf16[1024,256]{1,0:T(8,128)(2,1)S(1)} all-gather(bf16[128,256]{1,0:T(8,128)(2,1)S(1)} %copy-done.5), channel_id=1, replica_groups=mesh['sp'=8,'tp'=4] {'sp'}, dimensions={0}, use_global_device_ids=true | all-gather | bytes 589824 | tf_op jit(solution)/shard_map/all_gather | solution.py:86
  72.9 1.0 copy.59
  73.9 0.0 copy-start.3
  73.9 0.5 bitcast_reduce_fusion
  74.4 0.4 fusion.11
  74.7 0.2 copy-done.3
  74.9 0.5 fusion.16
  75.4 0.0 copy-start.8
  75.4 0.0 copy-start.6
  75.4 0.0 copy-start.1
  75.4 0.0 copy-start.7
  75.5 0.0 copy-done
  75.5 1.3 convolution_convert_fusion.1
  76.7 0.0 reduce-scatter.3.cloned.1.call-update
  76.8 0.0 all-gather.2.cloned.1.call-start
  76.8 0.0 copy-done.8
  76.8 0.1 copy.61
  76.9 0.1 eq.34
  77.0 0.1 fusion.24
  77.1 0.1 reduce_window_sum.11
  77.2 0.2 select_reduce_fusion.1
  77.4 0.1 reduce_sum.78
  77.5 0.1 copy.62
  77.6 0.0 copy-done.6
  77.6 0.1 convert_reduce_fusion
  77.7 20.1 %reduce-scatter.3.cloned.1.call-done = bf16[32,2048]{1,0:T(8,128)(2,1)} async-done(((bf16[128,2048]{1,0:T(8,128)(2,1)}), bf16[32,2048]{1,0:T(8,128)(2,1)}) %reduce-scatter.3.cloned.1.call-update) | async-done | bytes 131088 | tf_op jit(solution)/shard_map/reduce_scatter | solution.py:111
  97.8 0.0 copy-done.1
  97.8 1.1 multiply_reduce_fusion
  98.9 0.0 copy-done.7
  98.9 1.2 convolution_convert_fusion
  100.1 19.7 %all_to_all.10 = bf16[8,16,2048]{2,1,0:T(8,128)(2,1)} all-to-all(bf16[8,16,2048]{2,1,0:T(8,128)(2,1)S(1)} %bitcast.61), channel_id=1, replica_groups=mesh['sp'=8,'tp'=4] {'sp'}, dimensions={0} | all-to-all | bytes 1048576 | tf_op jit(solution)/shard_map/all_to_all | solution.py:146
  119.9 0.0 all-gather.2.cloned.1.call-update
  119.9 0.0 reduce-scatter.5.cloned.1.call-start
  119.9 20.8 %all-gather.2.cloned.1.call-done = bf16[512,2048]{1,0:T(8,128)(2,1)} async-done(((bf16[128,2048]{1,0:T(8,128)(2,1)}), bf16[512,2048]{1,0:T(8,128)(2,1)}) %all-gather.2.cloned.1.call-update) | async-done | bytes 2097168 | tf_op jit(solution)/shard_map/all_gather | solution.py:147
  140.7 6.5 %fusion.4 = f32[512,1024]{1,0:T(8,128)} fusion(bf16[512,2048]{1,0:T(8,128)(2,1)} %all-gather.2.cloned.1.call-done, bf16[1,2048,1024]{2,1,0:T(8,128)(2,1)} %param.23), kind=kOutput, calls=%fused_computation.4 | convolution fusion | flops 2147483648 | bytes 8388608 | tf_op jit(solution)/shard_map/dot_general | solution.py:148
  147.2 10.5 %fusion.6 = bf16[512,2048]{1,0:T(8,128)(2,1)} fusion(bf16[1,1024,2048]{2,1,0:T(8,128)(2,1)} %param.25, f32[512,1024]{1,0:T(8,128)} %fusion.4, bf16[512,2048]{1,0:T(8,128)(2,1)} %all-gather.2.cloned.1.call-done, bf16[1,2048,1024]{2,1,0:T(8,128)(2,1)} %param.24), kind=kOutput, calls=%fused_computation.6 | convolution fusion | flops 4299161600 | bytes 14680064 | tf_op jit(solution)/shard_map/dot_general | solution.py:153
  157.8 0.0 copy-start.2
  157.8 0.0 reduce-scatter.5.cloned.1.call-update
  157.8 31.3 %reduce-scatter.5.cloned.1.call-done = bf16[128,2048]{1,0:T(8,128)(2,1)} async-done(((bf16[512,2048]{1,0:T(8,128)(2,1)}), bf16[128,2048]{1,0:T(8,128)(2,1)}) %reduce-scatter.5.cloned.1.call-update) | async-done | bytes 524304 | tf_op jit(solution)/shard_map/reduce_scatter | solution.py:152
  189.1 19.9 %all_to_all.11 = bf16[8,16,2048]{2,1,0:T(8,128)(2,1)S(1)} all-to-all(bf16[8,16,2048]{2,1,0:T(8,128)(2,1)} %bitcast.65), channel_id=1, replica_groups=mesh['sp'=8,'tp'=4] {'sp'}, dimensions={0} | all-to-all | bytes 1048576 | tf_op jit(solution)/shard_map/all_to_all | solution.py:158
  209.0 0.0 copy-done.2
  209.0 1.0 fusion.9
  (11 shorter events, 0.2 us)
Async XLA Ops:
  6.5 68.9 %copy-start = (bf16[512,2048]{1,0:T(8,128)(2,1)S(1)}, bf16[512,2048]{1,0:T(8,128)(2,1)}, u32[]{:S(2)}) copy-start(bf16[512,2048]{1,0:T(8,128)(2,1)} %param.19) | copy-start | bytes 6291460
  6.5 3.8 %copy-start.4 = (bf16[128,512]{1,0:T(8,128)(2,1)S(1)}, bf16[128,512]{1,0:T(8,128)(2,1)}, u32[]{:S(2)}) copy-start(bf16[128,512]{1,0:T(8,128)(2,1)} %param.14) | copy-start | bytes 393220
  6.5 4.1 %copy-start.9 = (f32[128]{0:T(128)S(1)}, f32[128]{0:T(128)}, u32[]{:S(2)}) copy-start(f32[128]{0:T(128)} %param.17) | copy-start | bytes 1540
  6.5 91.3 %reduce-scatter.3.cloned.1.call-start = ((), (), s32[]{:S(2)}) async-start(), calls=%async_computation.4 | async-start | bytes 655360 | tf_op jit(solution)/shard_map/reduce_scatter | solution.py:111
  10.6 30.8 %copy-start.5 = (bf16[128,256]{1,0:T(8,128)(2,1)S(1)}, bf16[128,256]{1,0:T(8,128)(2,1)}, u32[]{:S(2)}) copy-start(bf16[128,256]{1,0:T(8,128)(2,1)} %param.16) | copy-start | bytes 196612
  73.9 1.0 copy-start.3
  75.4 1.4 copy-start.8
  75.4 2.1 copy-start.6
  75.4 22.4 %copy-start.1 = (bf16[32,2048]{1,0:T(8,128)(2,1)S(1)}, bf16[32,2048]{1,0:T(8,128)(2,1)}, u32[]{:S(2)}) copy-start(bf16[32,2048]{1,0:T(8,128)(2,1)} %param.13) | copy-start | bytes 393220
  75.4 23.4 %copy-start.7 = (f32[2048]{0:T(1024)S(1)}, f32[2048]{0:T(1024)}, u32[]{:S(2)}) copy-start(f32[2048]{0:T(1024)} %param.20) | copy-start | bytes 24580
  76.8 64.0 %all-gather.2.cloned.1.call-start = ((), (), s32[]{:S(2)}) async-start(), calls=%async_computation.5 | async-start | bytes 2621440 | tf_op jit(solution)/shard_map/all_gather | solution.py:147
  119.9 69.2 %reduce-scatter.5.cloned.1.call-start = ((), (), s32[]{:S(2)}) async-start(), calls=%async_computation.6 | async-start | bytes 2621440 | tf_op jit(solution)/shard_map/reduce_scatter | solution.py:152
  157.8 51.2 %copy-start.2 = (bf16[32,2048]{1,0:T(8,128)(2,1)S(1)}, bf16[32,2048]{1,0:T(8,128)(2,1)}, u32[]{:S(2)}) copy-start(bf16[32,2048]{1,0:T(8,128)(2,1)} %reduce-scatter.3.cloned.1.call-done) | copy-start | bytes 393220
Sparse Core Ops, SparseCore 0:
  76.9 20.8 reduce-scatter.2
  120.0 20.6 all-gather.1
  157.9 31.1 reduce-scatter.4
where the time goes:
time: 217 us
  blocking collectives  101 us (47%)
  waiting for transfers between devices  72.3 us (33%)
  matrix products  21.5 us (10%)
  between operations  13.4 us (6%)
  other arithmetic  5.78 us (3%)
  local copies, waits for them, and re-layouts  2.86 us (1%)
    all_gather x1, blocking collectives, local(): lax.all_gather(projected_value_heads, 'sp', axis=0, tiled=True)  31.4 us
    reduce_scatter x1, waiting for transfers between devices, local(): lax.psum_scatter(jnp.dot(row_block, down_matrix, preferred_element_type=j...  31.3 us
    all_gather x1, blocking collectives, local(): lax.all_gather(rotated_key_rows, 'sp', axis=0, tiled=True)  29.6 us
    all_gather x1, waiting for transfers between devices, local(): lax.all_gather(arrived.reshape(-1, model_width), 'tp', axis=0, tiled=True)  20.8 us
    reduce_scatter x1, waiting for transfers between devices, local(): lax.psum_scatter(jnp.dot(row_block, out_weight, preferred_element_type=jn...  20.1 us
    all_to_all x1, blocking collectives, local(): lax.all_to_all(expert_result.reshape(-1, capacity, model_width), 'sp', sp...  19.9 us
    all_to_all x1, blocking collectives, local(): lax.all_to_all(dispatch, 'sp', split_axis=0, concat_axis=0, tiled=True)  19.7 us
    dot_general x1, matrix products, local(): jnp.dot(row_block, down_matrix, preferred_element_type=jnp.float32)  10.5 us
  transfers between devices with their start and end apart: 3, of which 3 were waited for; matrix products, arithmetic and copies ran while one was open for 0% of the time, Pallas kernels for 0%

commit v1 on v0

--- a/solution.py
+++ b/solution.py
@@ -1,7 +1,14 @@
+import functools
+import math
+
 import jax
 import jax.numpy as jnp
 from jax import lax
+from jax.experimental import pallas as pl
+from jax.experimental.pallas import tpu as pltpu
 from jax.sharding import PartitionSpec as P
+
+MESH = pl.DeviceIdType.MESH
 
 HEAD_WIDTH = 128
 TOP = 2
@@ -53,7 +60,7 @@
     return turned.reshape(length, heads * head_size).astype(jnp.bfloat16)
 
 
-def local(
+def local_plain(
     x_resid,
     query_proj,
     projected_key_heads,
@@ -171,6 +178,519 @@
     return (middle + routed).astype(jnp.bfloat16)
 
 
+def rdma(src, dst, send_sem, recv_sem, device):
+    return pltpu.make_async_remote_copy(
+        src_ref=src,
+        dst_ref=dst,
+        send_sem=send_sem,
+        recv_sem=recv_sem,
+        device_id=device,
+        device_id_type=MESH,
+    )
+
+
+def turn_head(values, gain, cosine, sine):
+    values = values * lax.rsqrt(jnp.mean(values * values, axis=-1, keepdims=True) + NORM_EPS) * gain
+    width = values.shape[1]
+    quarter = width // 4
+    lane = lax.broadcasted_iota(jnp.int32, values.shape, 1)
+    swapped = jnp.where(
+        lane % (2 * quarter) < quarter,
+        pltpu.roll(values, width - quarter, 1),
+        pltpu.roll(values, quarter, 1),
+    )
+    return (values * cosine + swapped * sine).astype(jnp.bfloat16)
+
+
+def hop_order(count):
+    order = [0]
+    for distance in range(1, count // 2 + 1):
+        order.append(distance)
+        if count - distance != distance:
+            order.append(count - distance)
+    return order
+
+
+def layer_kernel(
+    n_sp,
+    n_tp,
+    capacity,
+    q_ref,
+    k_ref,
+    v_ref,
+    cos_ref,
+    sin_ref,
+    qg_ref,
+    kg_ref,
+    x_ref,
+    fg_ref,
+    route_ref,
+    score_ref,
+    ow_hbm,
+    wg_hbm,
+    wu_hbm,
+    wd_hbm,
+    out_ref,
+    kbuf,
+    vbuf,
+    qs,
+    att,
+    part,
+    rsbuf,
+    mid,
+    disp,
+    rows,
+    hid,
+    eo,
+    cor,
+    pair,
+    yrec,
+    res,
+    ret,
+    ow,
+    wg,
+    wu,
+    wd,
+    w_sem,
+    k_s,
+    k_r,
+    v_s,
+    v_r,
+    rs_s,
+    rs_r,
+    d_s,
+    rows_r,
+    y_s,
+    c_s,
+    e_s,
+    e_r,
+    p_s,
+    p_r,
+    b_s,
+    b_r,
+):
+    s = lax.axis_index("sp")
+    t = lax.axis_index("tp")
+    n_x = math.isqrt(n_sp // 2)
+    if n_x == 0 or n_sp % n_x:
+        n_x = 1
+    n_z = n_sp // n_x
+    z, x = s // n_x, s % n_x
+    n_y = n_tp // 2
+    y, c = t // 2, t % 2
+    core_peer = (s, y * 2 + 1 - c)
+    order = hop_order(n_sp)
+    seq_rows, q_width = q_ref.shape
+    kv_width = k_ref.shape[1]
+    q_heads, kv_heads = q_width // HEAD_WIDTH, kv_width // HEAD_WIDTH
+    groups = q_heads // kv_heads
+    own, model = x_ref.shape
+    f_width = wg.shape[1]
+    pending = []
+
+    def send(src, dst, send_sem, recv_sem, device):
+        copy = rdma(src, dst, send_sem, recv_sem, device)
+        copy.start()
+        pending.append(copy)
+
+    def arrive(dst, recv_sem):
+        rdma(dst, dst, recv_sem, recv_sem, core_peer).wait_recv()
+
+    weight_copies = [
+        pltpu.make_async_copy(ow_hbm, ow, w_sem.at[0]),
+        pltpu.make_async_copy(wg_hbm.at[0], wg, w_sem.at[1]),
+        pltpu.make_async_copy(wu_hbm.at[0], wu, w_sem.at[2]),
+        pltpu.make_async_copy(wd_hbm.at[0], wd, w_sem.at[3]),
+    ]
+    for copy in weight_copies:
+        copy.start()
+
+    barrier = pltpu.get_barrier_semaphore()
+    for d in range(1, n_sp):
+        pl.semaphore_signal(barrier, inc=1, device_id=((s + d) % n_sp, t), device_id_type=MESH)
+    for d in range(1, n_tp):
+        pl.semaphore_signal(barrier, inc=1, device_id=(s, (t + d) % n_tp), device_id_type=MESH)
+
+    cosine, sine = cos_ref[...], sin_ref[...]
+    for h in range(kv_heads):
+        cols = slice(h * HEAD_WIDTH, (h + 1) * HEAD_WIDTH)
+        kbuf[0, :, cols] = turn_head(k_ref[:, cols].astype(jnp.float32), kg_ref[...], cosine, sine)
+    pl.semaphore_wait(barrier, n_sp - 1 + n_tp - 1)
+
+    for buf, first, s_sem, r_sem in ((kbuf, kbuf.at[0], k_s, k_r), (vbuf, v_ref, v_s, v_r)):
+        for dx in range(1, n_x):
+            send(first, buf.at[dx], s_sem.at[dx], r_sem.at[dx], (z * n_x + (x + dx) % n_x, t))
+        for dz in range(1, n_z):
+            slot = dz * n_x
+            peer = ((z + dz) % n_z) * n_x + x
+            send(first, buf.at[slot], s_sem.at[slot], r_sem.at[slot], (peer, t))
+    vbuf[0] = v_ref[...]
+    for h in range(q_heads):
+        cols = slice(h * HEAD_WIDTH, (h + 1) * HEAD_WIDTH)
+        kv, member = h // groups, h % groups
+        qs[kv, member * seq_rows : (member + 1) * seq_rows, :] = turn_head(
+            q_ref[:, cols].astype(jnp.float32), qg_ref[...], cosine, sine
+        )
+    total_slots = n_sp * capacity
+    lane = lax.broadcasted_iota(jnp.int32, (own, total_slots), 1)
+    lane_place = lane // capacity
+    lane_expert = jnp.zeros_like(lane)
+    for k, d in enumerate(order):
+        lane_expert = jnp.where(lane_place == k, (s + d) % n_sp, lane_expert)
+    first_hit = route_ref[:, 0:1] == lane_expert
+    named = first_hit | (route_ref[:, 1:2] == lane_expert)
+    earlier = (
+        lax.broadcasted_iota(jnp.int32, (own, own), 1)
+        < lax.broadcasted_iota(jnp.int32, (own, own), 0)
+    )
+    rank = jnp.dot(
+        earlier.astype(jnp.float32).astype(jnp.bfloat16),
+        named.astype(jnp.float32).astype(jnp.bfloat16),
+        preferred_element_type=jnp.float32,
+    )
+    picked = jnp.where(
+        named & (rank == (lane % capacity).astype(jnp.float32)), 1.0, 0.0
+    )
+    route_scores = score_ref[...]
+    share = jnp.exp(route_scores - jnp.max(route_scores, axis=-1, keepdims=True))
+    share = share / jnp.sum(share, axis=-1, keepdims=True)
+    combiner = picked * jnp.where(first_hit, share[:, 0:1], share[:, 1:2])
+    picker = picked.astype(jnp.bfloat16)
+
+    for buf, s_sem, r_sem in ((kbuf, k_s, k_r), (vbuf, v_s, v_r)):
+        for dz in range(1, n_z):
+            slot = dz * n_x
+            arrive(buf.at[slot], r_sem.at[slot])
+            for dx in range(1, n_x):
+                send(
+                    buf.at[slot],
+                    buf.at[slot + dx],
+                    s_sem.at[slot + dx],
+                    r_sem.at[slot + dx],
+                    (z * n_x + (x + dx) % n_x, t),
+                )
+    for slot in range(n_sp):
+        if slot % n_x:
+            arrive(kbuf.at[slot], k_r.at[slot])
+    keys_all = n_sp * seq_rows
+    score_scale = HEAD_WIDTH ** (-0.5)
+    heads_done = []
+    for kv in range(kv_heads):
+        cols = slice(kv * HEAD_WIDTH, (kv + 1) * HEAD_WIDTH)
+        keys = kbuf[:, :, cols].reshape(keys_all, HEAD_WIDTH)
+        scores = (
+            lax.dot_general(
+                qs[kv], keys, (((1,), (1,)), ((), ())), preferred_element_type=jnp.float32
+            )
+            * score_scale
+        )
+        weights = jnp.exp(scores - jnp.max(scores, axis=-1, keepdims=True))
+        total = jnp.sum(weights, axis=-1, keepdims=True)
+        heads_done.append((weights.astype(jnp.bfloat16), total))
+    for slot in range(n_sp):
+        if slot % n_x:
+            arrive(vbuf.at[slot], v_r.at[slot])
+    for kv in range(kv_heads):
+        cols = slice(kv * HEAD_WIDTH, (kv + 1) * HEAD_WIDTH)
+        values = vbuf[:, :, cols].reshape(keys_all, HEAD_WIDTH)
+        weights, total = heads_done[kv]
+        mixed = jnp.dot(weights, values, preferred_element_type=jnp.float32) / total
+        for member in range(groups):
+            h = kv * groups + member
+            att[:, h * HEAD_WIDTH : (h + 1) * HEAD_WIDTH] = mixed[
+                member * seq_rows : (member + 1) * seq_rows
+            ].astype(jnp.bfloat16)
+
+    weight_copies[0].wait()
+    tile = min(512, model)
+    for j in range(model // tile):
+        cols = slice(j * tile, (j + 1) * tile)
+        part[:, :, cols] = (
+            jnp.dot(att[...], ow[:, cols], preferred_element_type=jnp.float32)
+            .astype(jnp.bfloat16)
+            .reshape(n_tp, own, tile)
+        )
+    for d in range(n_tp - 1, 0, -1):
+        peer = (t + d) % n_tp
+        send(part.at[peer], rsbuf.at[d], rs_s.at[d], rs_r.at[d], (s, peer))
+    summed = part[t].astype(jnp.float32)
+    for d in range(1, n_tp):
+        arrive(rsbuf.at[d], rs_r.at[d])
+        summed = summed + rsbuf[d].astype(jnp.float32)
+    middle = x_ref[...].astype(jnp.float32) + summed.astype(jnp.bfloat16).astype(jnp.float32)
+    mid[...] = middle
+    normed = (
+        middle
+        * lax.rsqrt(jnp.mean(middle * middle, axis=-1, keepdims=True) + NORM_EPS)
+        * fg_ref[...]
+    ).astype(jnp.bfloat16)
+    chosen = (
+        lax.dot_general(
+            picker, normed, (((0,), (0,)), ((), ())), preferred_element_type=jnp.float32
+        )
+        .astype(jnp.bfloat16)
+        .reshape(n_sp, capacity, model)
+    )
+    disp[...] = chosen
+    for k, d in enumerate(order):
+        if k:
+            send(disp.at[k], rows.at[k, t], d_s.at[k], rows_r.at[k, t], ((s + d) % n_sp, t))
+    rows[0, t] = chosen[0]
+
+    def forward(k):
+        if k:
+            arrive(rows.at[k, t], rows_r.at[k, t])
+        for dy in range(1, n_y):
+            peer = ((y + dy) % n_y) * 2 + c
+            send(rows.at[k, t], rows.at[k, t], y_s.at[k, dy], rows_r.at[k, t], (s, peer))
+        send(rows.at[k, t], rows.at[k, t], c_s.at[k, 0], rows_r.at[k, t], core_peer)
+
+    def relay(k):
+        for dy in range(1, n_y):
+            source = ((y + n_y - dy) % n_y) * 2 + c
+            arrive(rows.at[k, source], rows_r.at[k, source])
+            send(
+                rows.at[k, source],
+                rows.at[k, source],
+                c_s.at[k, dy],
+                rows_r.at[k, source],
+                core_peer,
+            )
+
+    def settle(k):
+        for dy in range(n_y):
+            source = ((y + n_y - dy) % n_y) * 2 + 1 - c
+            arrive(rows.at[k, source], rows_r.at[k, source])
+
+    n_groups = 2
+    group = n_sp // n_groups
+    group_rows = group * n_tp * capacity
+
+    def give_pair(g):
+        ks = pl.ds(g * group, group)
+        send(eo.at[1 - c, :, ks], cor.at[:, ks], e_s.at[g], e_r.at[g], core_peer)
+
+    def sum_pair(g):
+        ks = pl.ds(g * group, group)
+        arrive(cor.at[:, ks], e_r.at[g])
+        for dy in range(1, n_y):
+            far = (y + dy) % n_y
+            pair[dy, ks] = (
+                eo[c, far, ks].astype(jnp.float32) + cor[far, ks].astype(jnp.float32)
+            ).astype(jnp.bfloat16)
+            send(
+                pair.at[dy, ks], yrec.at[dy, ks], p_s.at[g, dy], p_r.at[g, dy], (s, far * 2 + c)
+            )
+
+    def give_back(g):
+        ks = pl.ds(g * group, group)
+        for dy in range(1, n_y):
+            arrive(yrec.at[dy, ks], p_r.at[g, dy])
+        for k in range(g * group, (g + 1) * group):
+            whole = eo[c, y, k].astype(jnp.float32) + cor[y, k].astype(jnp.float32)
+            for dy in range(1, n_y):
+                whole = whole + yrec[dy, k].astype(jnp.float32)
+            if k == 0:
+                ret[0] = whole.astype(jnp.bfloat16)
+            else:
+                res[k] = whole.astype(jnp.bfloat16)
+                peer = (s + n_sp - order[k]) % n_sp
+                send(res.at[k], ret.at[k], b_s.at[k], b_r.at[k], (peer, t))
+
+    def experts(g, hooks):
+        hooks = list(hooks)
+        block = rows[g * group : (g + 1) * group].reshape(group_rows, model)
+        f_tile = min(256, f_width)
+        for j in range(f_width // f_tile):
+            cols = slice(j * f_tile, (j + 1) * f_tile)
+            gate = jnp.dot(block, wg[:, cols], preferred_element_type=jnp.float32)
+            up = jnp.dot(block, wu[:, cols], preferred_element_type=jnp.float32)
+            hid[:, cols] = (gate / (1.0 + jnp.exp(-gate)) * up).astype(jnp.bfloat16)
+            if hooks:
+                hooks.pop(0)()
+        if g == 0:
+            weight_copies[3].wait()
+        for j in range(model // tile):
+            cols = slice(j * tile, (j + 1) * tile)
+            down = jnp.dot(hid[...], wd[:, cols], preferred_element_type=jnp.float32)
+            down = down.astype(jnp.bfloat16).reshape(group, n_y, 2, capacity, tile)
+            for core in range(2):
+                for far in range(n_y):
+                    eo[core, far, g * group : (g + 1) * group, :, cols] = down[:, far, core]
+            if hooks:
+                hooks.pop(0)()
+        for hook in hooks:
+            hook()
+
+    for k in range(group):
+        forward(k)
+    for k in range(group):
+        relay(k)
+    for k in range(group):
+        settle(k)
+    weight_copies[1].wait()
+    weight_copies[2].wait()
+    late = range(group, n_sp)
+    experts(
+        0,
+        [functools.partial(forward, k) for k in late] + [functools.partial(relay, k) for k in late],
+    )
+    give_pair(0)
+    for k in late:
+        settle(k)
+    nothing = lambda: None
+    experts(
+        1,
+        [
+            functools.partial(sum_pair, 0),
+            nothing,
+            nothing,
+            nothing,
+            functools.partial(give_back, 0),
+        ],
+    )
+    give_pair(1)
+    sum_pair(1)
+    give_back(1)
+    for k in range(1, n_sp):
+        arrive(ret.at[k], b_r.at[k])
+    high = combiner.astype(jnp.bfloat16)
+    rest = combiner - high.astype(jnp.float32)
+    middle_part = rest.astype(jnp.bfloat16)
+    low = (rest - middle_part.astype(jnp.float32)).astype(jnp.bfloat16)
+    returned = ret[...].reshape(total_slots, model)
+    routed = jnp.dot(
+        jnp.concatenate([high, middle_part, low], axis=0),
+        returned,
+        preferred_element_type=jnp.float32,
+    )
+    routed = routed[:own] + routed[own : 2 * own] + routed[2 * own :]
+    out_ref[...] = (mid[...] + routed).astype(jnp.bfloat16)
+    for copy in pending:
+        copy.wait_send()
+
+
+def rope_tables(token_positions):
+    row_angle, col_angle = grid_angles(token_positions, HEAD_WIDTH)
+    angles = jnp.concatenate([row_angle, row_angle, col_angle, col_angle], axis=1)
+    quarter = HEAD_WIDTH // 4
+    sign = jnp.where(jnp.arange(HEAD_WIDTH) % (2 * quarter) < quarter, -1.0, 1.0)
+    return jnp.cos(angles), jnp.sin(angles) * sign.astype(jnp.float32)
+
+
+def local(
+    x_resid,
+    query_proj,
+    projected_key_heads,
+    projected_value_heads,
+    query_gain,
+    key_norm_gain,
+    out_weight,
+    ffn_gain,
+    routing,
+    route_scores,
+    expert_gate,
+    expert_up,
+    expert_down,
+):
+    n_sp, n_tp = lax.axis_size("sp"), lax.axis_size("tp")
+    own, model = x_resid.shape
+    experts_all = n_sp * expert_gate.shape[0]
+    capacity = max(2, 2 * own * TOP // experts_all)
+    if capacity % 16 or n_tp % 2 or n_sp % 2 or expert_gate.shape[0] != 1:
+        return local_plain(
+            x_resid,
+            query_proj,
+            projected_key_heads,
+            projected_value_heads,
+            query_gain,
+            key_norm_gain,
+            out_weight,
+            ffn_gain,
+            routing,
+            route_scores,
+            expert_gate,
+            expert_up,
+            expert_down,
+        )
+    seq_rows, q_width = query_proj.shape
+    kv_width = projected_key_heads.shape[1]
+    kv_heads = kv_width // HEAD_WIDTH
+    groups = q_width // kv_width
+    f_width = expert_gate.shape[2]
+    n_y = n_tp // 2
+    token_positions = lax.axis_index("sp") * seq_rows + jnp.arange(seq_rows, dtype=jnp.int32)
+    cosine, sine = rope_tables(token_positions)
+    bf16 = jnp.bfloat16
+    dma = pltpu.SemaphoreType.DMA
+    vmem = pl.BlockSpec(memory_space=pltpu.VMEM)
+    hbm = pl.BlockSpec(memory_space=pl.ANY)
+    return pl.pallas_call(
+        functools.partial(layer_kernel, n_sp, n_tp, capacity),
+        out_shape=jax.ShapeDtypeStruct((own, model), bf16),
+        in_specs=[vmem] * 11 + [hbm] * 4,
+        out_specs=vmem,
+        scratch_shapes=[
+            pltpu.VMEM((n_sp, seq_rows, kv_width), bf16),
+            pltpu.VMEM((n_sp, seq_rows, kv_width), bf16),
+            pltpu.VMEM((kv_heads, groups * seq_rows, HEAD_WIDTH), bf16),
+            pltpu.VMEM((seq_rows, q_width), bf16),
+            pltpu.VMEM((n_tp, own, model), bf16),
+            pltpu.VMEM((n_tp, own, model), bf16),
+            pltpu.VMEM((own, model), jnp.float32),
+            pltpu.VMEM((n_sp, capacity, model), bf16),
+            pltpu.VMEM((n_sp, n_tp, capacity, model), bf16),
+            pltpu.VMEM((n_sp // 2 * n_tp * capacity, f_width), bf16),
+            pltpu.VMEM((2, n_y, n_sp, capacity, model), bf16),
+            pltpu.VMEM((n_y, n_sp, capacity, model), bf16),
+            pltpu.VMEM((n_y, n_sp, capacity, model), bf16),
+            pltpu.VMEM((n_y, n_sp, capacity, model), bf16),
+            pltpu.VMEM((n_sp, capacity, model), bf16),
+            pltpu.VMEM((n_sp, capacity, model), bf16),
+            pltpu.VMEM(out_weight.shape, bf16),
+            pltpu.VMEM(expert_gate.shape[1:], bf16),
+            pltpu.VMEM(expert_up.shape[1:], bf16),
+            pltpu.VMEM(expert_down.shape[1:], bf16),
+            dma((4,)),
+            dma((n_sp,)),
+            dma((n_sp,)),
+            dma((n_sp,)),
+            dma((n_sp,)),
+            dma((n_tp,)),
+            dma((n_tp,)),
+            dma((n_sp,)),
+            dma((n_sp, n_tp)),
+            dma((n_sp, n_y)),
+            dma((n_sp, n_y)),
+            dma((2,)),
+            dma((2,)),
+            dma((2, n_y)),
+            dma((2, n_y)),
+            dma((n_sp,)),
+            dma((n_sp,)),
+        ],
+        compiler_params=pltpu.CompilerParams(
+            collective_id=0, has_side_effects=True, vmem_limit_bytes=56 * 1024 * 1024
+        ),
+    )(
+        query_proj,
+        projected_key_heads,
+        projected_value_heads,
+        cosine,
+        sine,
+        query_gain.reshape(1, -1),
+        key_norm_gain.reshape(1, -1),
+        x_resid,
+        ffn_gain.reshape(1, -1),
+        routing,
+        route_scores,
+        out_weight,
+        expert_gate,
+        expert_up,
+        expert_down,
+    )
+
+
 def solution(mesh):
     in_specs = (
         P(("sp", "tp"), None),

time: 217 us -> 89.1 us (0.41)
  blocking collectives: 101 us -> 0 us
  Pallas kernels: 0 us -> 83.5 us
  waiting for transfers between devices: 72.3 us -> 0 us
  matrix products: 21.5 us -> 0 us
  between operations: 13.4 us -> 0.03 us
  other arithmetic: 5.78 us -> 1.13 us
    pallas_call x0 -> x1, Pallas kernels: none -> 83.5 us  [local(): pl.pallas_call(functools.partial(layer_kernel, n_sp, n_tp, capacity), out...]
    all_gather x2 -> x0, blocking collectives: 61 us -> none  [the longest x1 31.4 us: local(): lax.all_gather(projected_value_heads, 'sp', axis=0, tiled=True)]
    reduce_scatter x2 -> x0, waiting for transfers between devices: 51.4 us -> none  [the longest x1 31.3 us: local(): lax.psum_scatter(jnp.dot(row_block, down_matrix, preferred_element_type=j...]
    all_to_all x2 -> x0, blocking collectives: 39.6 us -> none  [the longest x1 19.9 us: local(): lax.all_to_all(expert_result.reshape(-1, capacity, model_width), 'sp', sp...]
    dot_general x7 -> x0, matrix products: 21.5 us -> none  [the longest x1 10.5 us: local(): jnp.dot(row_block, down_matrix, preferred_element_type=jnp.float32)]
    all_gather x1 -> x0, waiting for transfers between devices: 20.8 us -> none  [local(): lax.all_gather(arrived.reshape(-1, model_width), 'tp', axis=0, tiled=True)]
    unnamed x21 -> x3, local copies, waits for them, and re-layouts: 0.3 us -> 4.28 us
  transfers between devices with their start and end apart: 3 -> 0, of which waited for: 3 -> 0; matrix products, arithmetic and copies ran while one was open for 0% -> 0% of each run, Pallas kernels for 0% -> 0%
where the time goes in v1:
time: 89.1 us; the launch traced here: 88.9 us
  Pallas kernels  83.5 us (94%)
  local copies, waits for them, and re-layouts  4.28 us (5%)
  other arithmetic  1.13 us (1%)
    pallas_call x1, Pallas kernels, local(): pl.pallas_call(functools.partial(layer_kernel, n_sp, n_tp, capacity), out...  83.5 us
    unnamed x3, local copies, waits for them, and re-layouts  4.28 us

profile of v1, /device:TPU:0, one launch (start us, length us, event | category | flops | bytes accessed | tf_op | source)
XLA Modules:
  0.0 88.9 jit_solution(15474715336803019559)
XLA Ops:
  0.0 0.1 broadcast_multiply_fusion.1
  0.1 1.0 %sine_multiply_fusion = (f32[128,128]{1,0:T(8,128)}, f32[128,128]{1,0:T(8,128)}) fusion(f32[128]{0:T(128)S(1)} %compare_select_fusion, f32[128,32]{1,0:T(8,128)S(1)} %get-tuple-element.8, f32[128,32]{1,0:T(8,128)S(1)} %get-tuple-element.7), kind=kLoop, calls=%fused_computation.1 | loop fusion | flops 65536 | bytes 164352 | tf_op jit(solution)/shard_map/mul | solution.py:578
  1.1 1.4 %copy.14.route_ref = s32[32,2]{1,0:T(8,128)} copy(s32[32,2]{0,1:T(2,128)} %param.21) | data formatting | bytes 512 | tf_op args[8]
  2.5 1.4 %copy.15.score_ref = f32[32,2]{1,0:T(8,128)} copy(f32[32,2]{0,1:T(2,128)} %param.22) | data formatting | bytes 512 | tf_op args[9]
  3.9 83.5 %shard_map.127 = bf16[32,2048]{1,0:T(8,128)(2,1)} custom-call(bf16[128,512]{1,0:T(8,128)(2,1)} %q_ref.1, bf16[128,256]{1,0:T(8,128)(2,1)} %k_ref.1, bf16[128,256]{1,0:T(8,128)(2,1)} %v_ref.1, f32[128,128]{1,0:T(8,128)} %get-tuple-element.6.cos_ref, f32[128,128]{1,0:T(8,128)} %get-tuple-element.5.sin_ref, f32[1,128]{1,0:T(1,128)} %bitcast.4, ...), custom_call_target="tpu_custom_call" | custom-call | tf_op jit(solution)/shard_map/pallas_call | solution.py:628
  87.3 1.6 %copy.17 = bf16[32,2048]{1,0:T(8,128)(2,1)} copy(bf16[32,2048]{1,0:T(8,128)(2,1)} %shard_map.127) | data formatting | bytes 262144
  (3 shorter events, 0.0 us)

commit v2 on v1

--- a/solution.py
+++ b/solution.py
@@ -3,6 +3,7 @@
 
 import jax
 import jax.numpy as jnp
+import numpy as np
 from jax import lax
 from jax.experimental import pallas as pl
 from jax.experimental.pallas import tpu as pltpu
@@ -202,13 +203,19 @@
     return (values * cosine + swapped * sine).astype(jnp.bfloat16)
 
 
+def flip(index, mask):
+    bit = 1
+    while bit <= mask:
+        if mask // bit % 2:
+            index = index + bit * (1 - 2 * (index // bit % 2))
+        bit = bit * 2
+    return index
+
+
 def hop_order(count):
-    order = [0]
-    for distance in range(1, count // 2 + 1):
-        order.append(distance)
-        if count - distance != distance:
-            order.append(count - distance)
-    return order
+    half, quarter = count // 2, count // 4
+    near, far = list(range(half)), list(range(half, count))
+    return near[:quarter] + far + near[quarter:]
 
 
 def layer_kernel(
@@ -218,8 +225,7 @@
     q_ref,
     k_ref,
     v_ref,
-    cos_ref,
-    sin_ref,
+    freq_ref,
     qg_ref,
     kg_ref,
     x_ref,
@@ -275,7 +281,6 @@
     if n_x == 0 or n_sp % n_x:
         n_x = 1
     n_z = n_sp // n_x
-    z, x = s // n_x, s % n_x
     n_y = n_tp // 2
     y, c = t // 2, t % 2
     core_peer = (s, y * 2 + 1 - c)
@@ -311,19 +316,21 @@
     for d in range(1, n_tp):
         pl.semaphore_signal(barrier, inc=1, device_id=(s, (t + d) % n_tp), device_id_type=MESH)
 
-    cosine, sine = cos_ref[...], sin_ref[...]
+    table = (seq_rows, HEAD_WIDTH)
+    place = lax.broadcasted_iota(jnp.int32, table, 0) + s * seq_rows
+    column = lax.broadcasted_iota(jnp.int32, table, 1)
+    step = jnp.where(column < HEAD_WIDTH // 2, place // GRID_W, place % GRID_W)
+    angles = step.astype(jnp.float32) * freq_ref[...]
+    cosine, sine = jnp.cos(angles), jnp.sin(angles)
+    sine = jnp.where(column % (HEAD_WIDTH // 2) < HEAD_WIDTH // 4, -sine, sine)
     for h in range(kv_heads):
         cols = slice(h * HEAD_WIDTH, (h + 1) * HEAD_WIDTH)
         kbuf[0, :, cols] = turn_head(k_ref[:, cols].astype(jnp.float32), kg_ref[...], cosine, sine)
     pl.semaphore_wait(barrier, n_sp - 1 + n_tp - 1)
 
     for buf, first, s_sem, r_sem in ((kbuf, kbuf.at[0], k_s, k_r), (vbuf, v_ref, v_s, v_r)):
-        for dx in range(1, n_x):
-            send(first, buf.at[dx], s_sem.at[dx], r_sem.at[dx], (z * n_x + (x + dx) % n_x, t))
-        for dz in range(1, n_z):
-            slot = dz * n_x
-            peer = ((z + dz) % n_z) * n_x + x
-            send(first, buf.at[slot], s_sem.at[slot], r_sem.at[slot], (peer, t))
+        for slot in list(range(1, n_x)) + list(range(n_x, n_sp, n_x)):
+            send(first, buf.at[slot], s_sem.at[slot], r_sem.at[slot], (flip(s, slot), t))
     vbuf[0] = v_ref[...]
     for h in range(q_heads):
         cols = slice(h * HEAD_WIDTH, (h + 1) * HEAD_WIDTH)
@@ -332,29 +339,29 @@
             q_ref[:, cols].astype(jnp.float32), qg_ref[...], cosine, sine
         )
     total_slots = n_sp * capacity
-    lane = lax.broadcasted_iota(jnp.int32, (own, total_slots), 1)
-    lane_place = lane // capacity
-    lane_expert = jnp.zeros_like(lane)
+    slot_at = lax.broadcasted_iota(jnp.int32, (total_slots, own), 0)
+    slot_place = slot_at // capacity
+    slot_expert = jnp.zeros_like(slot_at)
     for k, d in enumerate(order):
-        lane_expert = jnp.where(lane_place == k, (s + d) % n_sp, lane_expert)
-    first_hit = route_ref[:, 0:1] == lane_expert
-    named = first_hit | (route_ref[:, 1:2] == lane_expert)
+        slot_expert = jnp.where(slot_place == k, flip(s, d), slot_expert)
+    first_hit = route_ref[0:1, :] == slot_expert
+    named = first_hit | (route_ref[1:2, :] == slot_expert)
     earlier = (
-        lax.broadcasted_iota(jnp.int32, (own, own), 1)
-        < lax.broadcasted_iota(jnp.int32, (own, own), 0)
+        lax.broadcasted_iota(jnp.int32, (own, own), 0)
+        < lax.broadcasted_iota(jnp.int32, (own, own), 1)
     )
     rank = jnp.dot(
+        named.astype(jnp.float32).astype(jnp.bfloat16),
         earlier.astype(jnp.float32).astype(jnp.bfloat16),
-        named.astype(jnp.float32).astype(jnp.bfloat16),
         preferred_element_type=jnp.float32,
     )
     picked = jnp.where(
-        named & (rank == (lane % capacity).astype(jnp.float32)), 1.0, 0.0
+        named & (rank == (slot_at % capacity).astype(jnp.float32)), 1.0, 0.0
     )
     route_scores = score_ref[...]
-    share = jnp.exp(route_scores - jnp.max(route_scores, axis=-1, keepdims=True))
-    share = share / jnp.sum(share, axis=-1, keepdims=True)
-    combiner = picked * jnp.where(first_hit, share[:, 0:1], share[:, 1:2])
+    share = jnp.exp(route_scores - jnp.max(route_scores, axis=0, keepdims=True))
+    share = share / jnp.sum(share, axis=0, keepdims=True)
+    combiner = picked * jnp.where(first_hit, share[0:1, :], share[1:2, :])
     picker = picked.astype(jnp.bfloat16)
 
     for buf, s_sem, r_sem in ((kbuf, k_s, k_r), (vbuf, v_s, v_r)):
@@ -367,7 +374,7 @@
                     buf.at[slot + dx],
                     s_sem.at[slot + dx],
                     r_sem.at[slot + dx],
-                    (z * n_x + (x + dx) % n_x, t),
+                    (flip(s, dx), t),
                 )
     for slot in range(n_sp):
         if slot % n_x:
@@ -411,7 +418,7 @@
             .reshape(n_tp, own, tile)
         )
     for d in range(n_tp - 1, 0, -1):
-        peer = (t + d) % n_tp
+        peer = flip(t, d)
         send(part.at[peer], rsbuf.at[d], rs_s.at[d], rs_r.at[d], (s, peer))
     summed = part[t].astype(jnp.float32)
     for d in range(1, n_tp):
@@ -425,16 +432,14 @@
         * fg_ref[...]
     ).astype(jnp.bfloat16)
     chosen = (
-        lax.dot_general(
-            picker, normed, (((0,), (0,)), ((), ())), preferred_element_type=jnp.float32
-        )
+        jnp.dot(picker, normed, preferred_element_type=jnp.float32)
         .astype(jnp.bfloat16)
         .reshape(n_sp, capacity, model)
     )
     disp[...] = chosen
     for k, d in enumerate(order):
         if k:
-            send(disp.at[k], rows.at[k, t], d_s.at[k], rows_r.at[k, t], ((s + d) % n_sp, t))
+            send(disp.at[k], rows.at[k, t], d_s.at[k], rows_r.at[k, t], (flip(s, d), t))
     rows[0, t] = chosen[0]
 
     def forward(k):
@@ -471,31 +476,27 @@
         send(eo.at[1 - c, :, ks], cor.at[:, ks], e_s.at[g], e_r.at[g], core_peer)
 
     def sum_pair(g):
-        ks = pl.ds(g * group, group)
-        arrive(cor.at[:, ks], e_r.at[g])
+        arrive(cor.at[:, pl.ds(g * group, group)], e_r.at[g])
+        for k in range(group - 1, -1, -1) if g == 0 else range(group, n_sp):
+            for dy in range(1, n_y):
+                far = (y + dy) % n_y
+                pair[dy, k] = (
+                    eo[c, far, k].astype(jnp.float32) + cor[far, k].astype(jnp.float32)
+                ).astype(jnp.bfloat16)
+                send(
+                    pair.at[dy, k], yrec.at[dy, k], p_s.at[k, dy], p_r.at[k, dy], (s, far * 2 + c)
+                )
+
+    def give_back(k):
+        whole = eo[c, y, k].astype(jnp.float32) + cor[y, k].astype(jnp.float32)
         for dy in range(1, n_y):
-            far = (y + dy) % n_y
-            pair[dy, ks] = (
-                eo[c, far, ks].astype(jnp.float32) + cor[far, ks].astype(jnp.float32)
-            ).astype(jnp.bfloat16)
-            send(
-                pair.at[dy, ks], yrec.at[dy, ks], p_s.at[g, dy], p_r.at[g, dy], (s, far * 2 + c)
-            )
-
-    def give_back(g):
-        ks = pl.ds(g * group, group)
-        for dy in range(1, n_y):
-            arrive(yrec.at[dy, ks], p_r.at[g, dy])
-        for k in range(g * group, (g + 1) * group):
-            whole = eo[c, y, k].astype(jnp.float32) + cor[y, k].astype(jnp.float32)
-            for dy in range(1, n_y):
-                whole = whole + yrec[dy, k].astype(jnp.float32)
-            if k == 0:
-                ret[0] = whole.astype(jnp.bfloat16)
-            else:
-                res[k] = whole.astype(jnp.bfloat16)
-                peer = (s + n_sp - order[k]) % n_sp
-                send(res.at[k], ret.at[k], b_s.at[k], b_r.at[k], (peer, t))
+            arrive(yrec.at[dy, k], p_r.at[k, dy])
+            whole = whole + yrec[dy, k].astype(jnp.float32)
+        if k == 0:
+            ret[0] = whole.astype(jnp.bfloat16)
+        else:
+            res[k] = whole.astype(jnp.bfloat16)
+            send(res.at[k], ret.at[k], b_s.at[k], b_r.at[k], (flip(s, order[k]), t))
 
     def experts(g, hooks):
         hooks = list(hooks)
@@ -539,19 +540,12 @@
     for k in late:
         settle(k)
     nothing = lambda: None
-    experts(
-        1,
-        [
-            functools.partial(sum_pair, 0),
-            nothing,
-            nothing,
-            nothing,
-            functools.partial(give_back, 0),
-        ],
-    )
+    early = [functools.partial(give_back, k) for k in (*range(group - 1, -1, -1),)]
+    experts(1, [functools.partial(sum_pair, 0), nothing, nothing] + early)
     give_pair(1)
     sum_pair(1)
-    give_back(1)
+    for k in late:
+        give_back(k)
     for k in range(1, n_sp):
         arrive(ret.at[k], b_r.at[k])
     high = combiner.astype(jnp.bfloat16)
@@ -559,23 +553,20 @@
     middle_part = rest.astype(jnp.bfloat16)
     low = (rest - middle_part.astype(jnp.float32)).astype(jnp.bfloat16)
     returned = ret[...].reshape(total_slots, model)
-    routed = jnp.dot(
-        jnp.concatenate([high, middle_part, low], axis=0),
-        returned,
-        preferred_element_type=jnp.float32,
-    )
-    routed = routed[:own] + routed[own : 2 * own] + routed[2 * own :]
-    out_ref[...] = (mid[...] + routed).astype(jnp.bfloat16)
+    routed = jnp.zeros((own, model), jnp.float32)
+    for piece in (high, middle_part, low):
+        routed = routed + lax.dot_general(
+            piece, returned, (((0,), (0,)), ((), ())), preferred_element_type=jnp.float32
+        )
+    out_ref[...] = mid[...] + routed
     for copy in pending:
         copy.wait_send()
 
 
-def rope_tables(token_positions):
-    row_angle, col_angle = grid_angles(token_positions, HEAD_WIDTH)
-    angles = jnp.concatenate([row_angle, row_angle, col_angle, col_angle], axis=1)
+def head_frequency():
     quarter = HEAD_WIDTH // 4
-    sign = jnp.where(jnp.arange(HEAD_WIDTH) % (2 * quarter) < quarter, -1.0, 1.0)
-    return jnp.cos(angles), jnp.sin(angles) * sign.astype(jnp.float32)
+    frequency = ROPE_BASE ** (-np.arange(quarter, dtype=np.float32) / quarter)
+    return jnp.asarray(np.tile(frequency, 4).reshape(1, HEAD_WIDTH), jnp.float32)
 
 
 def local(
@@ -597,7 +588,7 @@
     own, model = x_resid.shape
     experts_all = n_sp * expert_gate.shape[0]
     capacity = max(2, 2 * own * TOP // experts_all)
-    if capacity % 16 or n_tp % 2 or n_sp % 2 or expert_gate.shape[0] != 1:
+    if capacity % 16 or n_tp & (n_tp - 1) or n_sp & (n_sp - 1) or n_tp < 2 or n_sp < 4 or expert_gate.shape[0] != 1:
         return local_plain(
             x_resid,
             query_proj,
@@ -619,16 +610,14 @@
     groups = q_width // kv_width
     f_width = expert_gate.shape[2]
     n_y = n_tp // 2
-    token_positions = lax.axis_index("sp") * seq_rows + jnp.arange(seq_rows, dtype=jnp.int32)
-    cosine, sine = rope_tables(token_positions)
     bf16 = jnp.bfloat16
     dma = pltpu.SemaphoreType.DMA
     vmem = pl.BlockSpec(memory_space=pltpu.VMEM)
     hbm = pl.BlockSpec(memory_space=pl.ANY)
     return pl.pallas_call(
         functools.partial(layer_kernel, n_sp, n_tp, capacity),
-        out_shape=jax.ShapeDtypeStruct((own, model), bf16),
-        in_specs=[vmem] * 11 + [hbm] * 4,
+        out_shape=jax.ShapeDtypeStruct((own, model), jnp.float32),
+        in_specs=[vmem] * 10 + [hbm] * 4,
         out_specs=vmem,
         scratch_shapes=[
             pltpu.VMEM((n_sp, seq_rows, kv_width), bf16),
@@ -664,8 +653,8 @@
             dma((n_sp, n_y)),
             dma((2,)),
             dma((2,)),
-            dma((2, n_y)),
-            dma((2, n_y)),
+            dma((n_sp, n_y)),
+            dma((n_sp, n_y)),
             dma((n_sp,)),
             dma((n_sp,)),
         ],
@@ -676,19 +665,18 @@
         query_proj,
         projected_key_heads,
         projected_value_heads,
-        cosine,
-        sine,
+        head_frequency(),
         query_gain.reshape(1, -1),
         key_norm_gain.reshape(1, -1),
         x_resid,
         ffn_gain.reshape(1, -1),
-        routing,
-        route_scores,
+        routing.T,
+        route_scores.T,
         out_weight,
         expert_gate,
         expert_up,
         expert_down,
-    )
+    ).astype(bf16)
 
 
 def solution(mesh):

time: 89.1 us -> 78.8 us (0.88)
  Pallas kernels: 83.5 us -> 77 us
  local copies, waits for them, and re-layouts: 4.28 us -> 0 us
    pallas_call x1, Pallas kernels: 83.5 us -> 77 us  [local(): pl.pallas_call(functools.partial(layer_kernel, n_sp, n_tp, capacity), out...]
    unnamed x3 -> x0, local copies, waits for them, and re-layouts: 4.28 us -> none
    convert_element_type x1, other arithmetic: 0.01 us -> 1.62 us  [local(): return pl.pallas_call(functools.partial(layer_kernel, n_sp, n_tp, capacit...]
    mul x2 -> x0, other arithmetic: 1.1 us -> none  [the longest x1 1 us: rope_tables(): return (jnp.cos(angles), jnp.sin(angles) * sign.astype(jnp.float32))]
where the time goes in v2:
time: 78.8 us; the launch traced here: 78.6 us
  Pallas kernels  77 us (98%)
  other arithmetic  1.62 us (2%)
    pallas_call x1, Pallas kernels, local(): pl.pallas_call(functools.partial(layer_kernel, n_sp, n_tp, capacity), out...  77 us
    convert_element_type x1, other arithmetic, local(): return pl.pallas_call(functools.partial(layer_kernel, n_sp, n_tp, capacit...  1.62 us

profile of v2, /device:TPU:0, one launch (start us, length us, event | category | flops | bytes accessed | tf_op | source)
XLA Modules:
  0.0 78.6 jit_solution(1711717183509282990)
XLA Ops:
  0.0 77.0 %shard_map.136 = f32[32,2048]{1,0:T(8,128)} custom-call(bf16[128,512]{1,0:T(8,128)(2,1)} %q_ref.1, bf16[128,256]{1,0:T(8,128)(2,1)} %k_ref.1, bf16[128,256]{1,0:T(8,128)(2,1)} %v_ref.1, f32[1,128]{1,0:T(1,128)} %constant.2.clone.freq_ref, f32[1,128]{1,0:T(1,128)} %bitcast.8, f32[1,128]{1,0:T(1,128)} %bitcast.9, bf16[32,2048]{1,0:T(8,128)(2,1)} %x_ref.1, ...), custom_call_target="tpu_custom_call" | custom-call | tf_op jit(solution)/shard_map/pallas_call | solution.py:617
  77.0 1.6 %convert_element_type.3 = bf16[32,2048]{1,0:T(8,128)(2,1)} convert(f32[32,2048]{1,0:T(8,128)} %shard_map.136) | non-fusion elementwise | flops 65536 | bytes 393216 | tf_op jit(solution)/shard_map/convert_element_type | solution.py:679

commit v3 on v2

--- a/solution.py
+++ b/solution.py
@@ -328,9 +328,14 @@
         kbuf[0, :, cols] = turn_head(k_ref[:, cols].astype(jnp.float32), kg_ref[...], cosine, sine)
     pl.semaphore_wait(barrier, n_sp - 1 + n_tp - 1)
 
-    for buf, first, s_sem, r_sem in ((kbuf, kbuf.at[0], k_s, k_r), (vbuf, v_ref, v_s, v_r)):
-        for slot in list(range(1, n_x)) + list(range(n_x, n_sp, n_x)):
-            send(first, buf.at[slot], s_sem.at[slot], r_sem.at[slot], (flip(s, slot), t))
+    for slot in list(range(1, n_x)) + list(range(n_x, n_sp, n_x)):
+        send(kbuf.at[0], kbuf.at[slot], k_s.at[slot], k_r.at[slot], (flip(s, slot), t))
+
+    def send_values(slot):
+        send(v_ref, vbuf.at[slot], v_s.at[slot], v_r.at[slot], (flip(s, slot), t))
+
+    for slot in range(1, n_x):
+        send_values(slot)
     vbuf[0] = v_ref[...]
     for h in range(q_heads):
         cols = slice(h * HEAD_WIDTH, (h + 1) * HEAD_WIDTH)
@@ -376,6 +381,8 @@
                     r_sem.at[slot + dx],
                     (flip(s, dx), t),
                 )
+            if buf is kbuf:
+                send_values(slot)
     for slot in range(n_sp):
         if slot % n_x:
             arrive(kbuf.at[slot], k_r.at[slot])
@@ -437,9 +444,13 @@
         .reshape(n_sp, capacity, model)
     )
     disp[...] = chosen
-    for k, d in enumerate(order):
-        if k:
-            send(disp.at[k], rows.at[k, t], d_s.at[k], rows_r.at[k, t], (flip(s, d), t))
+
+    def dispatch(k):
+        send(disp.at[k], rows.at[k, t], d_s.at[k], rows_r.at[k, t], (flip(s, order[k]), t))
+
+    window = n_sp // 2
+    for k in range(1, window):
+        dispatch(k)
     rows[0, t] = chosen[0]
 
     def forward(k):
@@ -475,17 +486,23 @@
         ks = pl.ds(g * group, group)
         send(eo.at[1 - c, :, ks], cor.at[:, ks], e_s.at[g], e_r.at[g], core_peer)
 
-    def sum_pair(g):
+    def sum_pair(k):
+        for dy in range(1, n_y):
+            far = (y + dy) % n_y
+            pair[dy, k] = (
+                eo[c, far, k].astype(jnp.float32) + cor[far, k].astype(jnp.float32)
+            ).astype(jnp.bfloat16)
+            send(pair.at[dy, k], yrec.at[dy, k], p_s.at[k, dy], p_r.at[k, dy], (s, far * 2 + c))
+
+    def start_pairs(g, slots):
         arrive(cor.at[:, pl.ds(g * group, group)], e_r.at[g])
-        for k in range(group - 1, -1, -1) if g == 0 else range(group, n_sp):
-            for dy in range(1, n_y):
-                far = (y + dy) % n_y
-                pair[dy, k] = (
-                    eo[c, far, k].astype(jnp.float32) + cor[far, k].astype(jnp.float32)
-                ).astype(jnp.bfloat16)
-                send(
-                    pair.at[dy, k], yrec.at[dy, k], p_s.at[k, dy], p_r.at[k, dy], (s, far * 2 + c)
-                )
+        for k in slots[:2]:
+            sum_pair(k)
+
+    def return_next(i, slots):
+        give_back(slots[i])
+        if i + 2 < len(slots):
+            sum_pair(slots[i + 2])
 
     def give_back(k):
         whole = eo[c, y, k].astype(jnp.float32) + cor[y, k].astype(jnp.float32)
@@ -525,6 +542,9 @@
 
     for k in range(group):
         forward(k)
+        if k:
+            dispatch(window + k - 1)
+    dispatch(n_sp - 1)
     for k in range(group):
         relay(k)
     for k in range(group):
@@ -540,12 +560,16 @@
     for k in late:
         settle(k)
     nothing = lambda: None
-    early = [functools.partial(give_back, k) for k in (*range(group - 1, -1, -1),)]
-    experts(1, [functools.partial(sum_pair, 0), nothing, nothing] + early)
+    early = list(range(group - 1, -1, -1))
+    experts(
+        1,
+        [functools.partial(start_pairs, 0, early), nothing, nothing, nothing]
+        + [functools.partial(return_next, i, early) for i in range(group)],
+    )
     give_pair(1)
-    sum_pair(1)
-    for k in late:
-        give_back(k)
+    start_pairs(1, late)
+    for i in range(group):
+        return_next(i, late)
     for k in range(1, n_sp):
         arrive(ret.at[k], b_r.at[k])
     high = combiner.astype(jnp.bfloat16)

time: 78.8 us -> 78.2 us (level)
  Pallas kernels: 77 us -> 76.2 us
where the time goes in v3:
time: 78.2 us; the launch traced here: 77.9 us
  Pallas kernels  76.2 us (97%)
  other arithmetic  1.62 us (2%)
    pallas_call x1, Pallas kernels, local(): pl.pallas_call(functools.partial(layer_kernel, n_sp, n_tp, capacity), out...  76.2 us
    convert_element_type x1, other arithmetic, local(): return pl.pallas_call(functools.partial(layer_kernel, n_sp, n_tp, capacit...  1.62 us

profile of v3, /device:TPU:0, one launch (start us, length us, event | category | flops | bytes accessed | tf_op | source)
XLA Modules:
  0.0 77.9 jit_solution(17201361455640703882)
XLA Ops:
  0.0 76.2 %shard_map.136 = f32[32,2048]{1,0:T(8,128)} custom-call(bf16[128,512]{1,0:T(8,128)(2,1)} %q_ref.1, bf16[128,256]{1,0:T(8,128)(2,1)} %k_ref.1, bf16[128,256]{1,0:T(8,128)(2,1)} %v_ref.1, f32[1,128]{1,0:T(1,128)} %constant.2.clone.freq_ref, f32[1,128]{1,0:T(1,128)} %bitcast.8, f32[1,128]{1,0:T(1,128)} %bitcast.9, bf16[32,2048]{1,0:T(8,128)(2,1)} %x_ref.1, ...), custom_call_target="tpu_custom_call" | custom-call | tf_op jit(solution)/shard_map/pallas_call | solution.py:641
  76.2 1.6 %convert_element_type.3 = bf16[32,2048]{1,0:T(8,128)(2,1)} convert(f32[32,2048]{1,0:T(8,128)} %shard_map.136) | non-fusion elementwise | flops 65536 | bytes 393216 | tf_op jit(solution)/shard_map/convert_element_type | solution.py:703
